TPU v7x, 32 devices: a whole 2x2x4 slice. The times are simulated.
32 devices in a mesh: sp: 16 (over z, y, x), tp: 2 (over core).
Axes of the slice: x: 2, y: 2, z: 4, core: 2. Of those that a mesh axis runs over, the one named last changes fastest.
Arguments:
- x_rows: bfloat16 [2048, 2048], P('sp'), may hold values from -6 to 6
- queries: bfloat16 [2048, 1024], P('sp', 'tp'), may hold values from -8 to 8
- keys: bfloat16 [2048, 512], P('sp', 'tp'), may hold values from -8 to 8
- values: bfloat16 [2048, 512], P('sp', 'tp'), may hold values from -6 to 6
- query_norm_gain: float32 [64], replicated, may hold values from 1 to 8
- key_norm_gain: float32 [64], replicated, may hold values from 1 to 8
- out_weight: bfloat16 [1024, 2048], P('tp'), may hold values from -0.1875 to 0.1875
- ffn_gain: float32 [2048], replicated, may hold values from 0.1 to 1.9
- gate_weight: bfloat16 [2048, 5120], P('sp', 'tp'), may hold values from -0.125 to 0.125
- value_weight: bfloat16 [2048, 5120], P('sp', 'tp'), may hold values from -0.125 to 0.125
- conv_gate: float32 [3, 5120], P(None, 'tp'), may hold values from -3.5 to 3.5
- conv_value: float32 [3, 5120], P(None, 'tp'), may hold values from -3.5 to 3.5
- down_weight: bfloat16 [2048, 5120], P('sp', 'tp'), may hold values from -0.078125 to 0.078125
Outputs:
- layer_out: bfloat16 [2048, 2048], P('sp')
All inputs are finite; a program needn't handle non-finite values.
Results may differ from a plain program's by a relative error of at most 0.017.
Values may be sent and summed in bfloat16 or wider, within the bound.
A program may use at most 64 MiB of HBM per device.

v0:
```python
import math
import jax
import jax.numpy as jnp
from jax import lax
from jax.sharding import PartitionSpec as P

HEAD_SIZE = 64
GRID_ROW_WIDTH = 64
eps_norm = 1e-06
theta = 10000.0


def with_halo(cells, sides, width):
    for axis, dim in sides:
        count = lax.axis_size(axis)
        ends = count - 1
        head = lax.slice_in_dim(cells, 0, width, axis=dim)
        tail = lax.slice_in_dim(cells, cells.shape[dim] - width, cells.shape[dim], axis=dim)
        cells = jnp.concatenate(
            [
                lax.ppermute(tail, axis, [(i, (i + 1) % count) for i in range(ends)]),
                cells,
                lax.ppermute(head, axis, [((i + 1) % count, i) for i in range(ends)]),
            ],
            axis=dim,
        )
    return cells


def per_head_norm(head_block, gain_vec):
    wide_vals = head_block.astype(jnp.float32)
    inverse_rms = lax.rsqrt(jnp.mean(wide_vals * wide_vals, axis=-1, keepdims=True) + eps_norm)
    return wide_vals * inverse_rms * gain_vec


def turn_half(half_vec, places):
    quarter_len = half_vec.shape[-1] // 2
    inverse_rates = 1.0 / theta ** (
        jnp.arange(quarter_len, dtype=jnp.float32) * 2.0 / half_vec.shape[-1]
    )
    angles = places.astype(jnp.float32)[:, None] * inverse_rates[None, :]
    angles = jnp.concatenate([angles, angles], axis=-1)[:, None, :]
    front_part = half_vec[..., :quarter_len]
    back_part = half_vec[..., quarter_len:]
    return half_vec * jnp.cos(angles) + jnp.concatenate(
        [-back_part, front_part], axis=-1
    ) * jnp.sin(angles)


def apply_rotary(normed_heads, token_positions):
    half_point = normed_heads.shape[-1] // 2
    grid_row = token_positions // GRID_ROW_WIDTH
    grid_col = token_positions % GRID_ROW_WIDTH
    return jnp.concatenate(
        [
            turn_half(normed_heads[..., :half_point], grid_row),
            turn_half(normed_heads[..., half_point:], grid_col),
        ],
        axis=-1,
    )


def row_norm(rows_wide, gain_vec):
    inverse_rms = lax.rsqrt(jnp.mean(rows_wide * rows_wide, axis=-1, keepdims=True) + eps_norm)
    return (rows_wide * inverse_rms * gain_vec).astype(jnp.bfloat16)


def contract_units(left_rows, right_rows):
    return lax.dot_general(
        left_rows, right_rows, (((1,), (1,)), ((), ())), preferred_element_type=jnp.float32
    )


def shards(
    x_rows,
    queries,
    keys,
    values,
    query_norm_gain,
    key_norm_gain,
    out_weight,
    ffn_gain,
    gate_weight,
    value_weight,
    conv_gate,
    conv_value,
    down_weight,
):
    collected = (
        lax.all_gather(gate_weight, "sp", axis=0, tiled=True),
        lax.all_gather(value_weight, "sp", axis=0, tiled=True),
        lax.all_gather(down_weight, "sp", axis=0, tiled=True),
    )
    tokens_here = queries.shape[0]
    query_heads = queries.shape[1] // HEAD_SIZE
    key_heads = keys.shape[1] // HEAD_SIZE
    group_width = query_heads // key_heads
    lane_rows = group_width * tokens_here
    token_positions = lax.axis_index("sp") * tokens_here + jnp.arange(tokens_here, dtype=jnp.int32)
    rotated_queries = apply_rotary(
        per_head_norm(queries.reshape(tokens_here, query_heads, HEAD_SIZE), query_norm_gain),
        token_positions,
    )
    query_lanes = rotated_queries.reshape(tokens_here, key_heads, group_width, HEAD_SIZE).transpose(
        1, 2, 0, 3
    )
    query_lanes = query_lanes.reshape(key_heads, lane_rows, HEAD_SIZE) * HEAD_SIZE ** (-0.5)
    start_state = (
        jnp.full((key_heads, lane_rows), -1e30, jnp.float32),
        jnp.zeros((key_heads, lane_rows), jnp.float32),
        jnp.zeros((key_heads, lane_rows, HEAD_SIZE), jnp.float32),
    )
    key_piece = lax.all_gather(keys, "sp", axis=0, tiled=True)
    value_piece = lax.all_gather(values, "sp", axis=0, tiled=True)
    row_count = key_piece.shape[0]
    key_places = jnp.arange(row_count, dtype=jnp.int32)
    turned = apply_rotary(
        per_head_norm(key_piece.reshape(row_count, key_heads, HEAD_SIZE), key_norm_gain), key_places
    )
    key_span = math.gcd(row_count, 2048)
    span_count = row_count // key_span
    turned = turned.reshape(span_count, key_span, key_heads, HEAD_SIZE)
    value_matrix = value_piece.reshape(span_count, key_span, key_heads, HEAD_SIZE)

    def one_span(state_now, inputs):
        running_top, denominator, weighted = state_now
        key_block, value_block = inputs
        scores = jnp.einsum("hrd,shd->hrs", query_lanes, key_block, precision=lax.Precision.HIGHEST)
        new_top = jnp.maximum(running_top, jnp.max(scores, axis=-1))
        factor = jnp.exp(running_top - new_top)
        weights = jnp.exp(scores - new_top[..., None])
        denominator = denominator * factor + jnp.sum(weights, axis=-1)
        weighted = weighted * factor[..., None] + jnp.einsum(
            "hrs,shd->hrd",
            weights.astype(jnp.bfloat16),
            value_block,
            preferred_element_type=jnp.float32,
        )
        return ((new_top, denominator, weighted), None)

    folded_state, _ = lax.scan(one_span, start_state, (turned, value_matrix))
    running_top, denominator, weighted = folded_state
    attended = (weighted / denominator[..., None]).reshape(
        key_heads, group_width, tokens_here, HEAD_SIZE
    )
    attended = (
        attended.transpose(2, 0, 1, 3)
        .reshape(tokens_here, query_heads * HEAD_SIZE)
        .astype(jnp.bfloat16)
    )
    share_rows = tokens_here // lax.axis_size("tp")
    head_share = lax.psum_scatter(
        jnp.dot(attended, out_weight, preferred_element_type=jnp.float32).astype(jnp.bfloat16),
        "tp",
        scatter_dimension=0,
        tiled=True,
    ).astype(jnp.float32)
    own_rows = lax.dynamic_slice_in_dim(x_rows, lax.axis_index("tp") * share_rows, share_rows, 0)
    middle_rows = own_rows.astype(jnp.float32) + head_share
    normed = lax.all_gather(row_norm(middle_rows, ffn_gain), "tp", axis=0, tiled=True)
    unit_local = gate_weight.shape[1]
    gate_pre = jnp.dot(normed, collected[0], preferred_element_type=jnp.float32).astype(
        jnp.bfloat16
    )
    value_pre = jnp.dot(normed, collected[1], preferred_element_type=jnp.float32).astype(
        jnp.bfloat16
    )
    joined = jnp.concatenate([gate_pre, value_pre], axis=1)
    padded = with_halo(joined, (("sp", 0),), 1).astype(jnp.float32)
    conv_taps = jnp.concatenate([conv_gate, conv_value], axis=1)
    convolved = conv_taps[0] * padded[:-2] + conv_taps[1] * padded[1:-1] + conv_taps[2] * padded[2:]
    hidden = (jax.nn.silu(convolved[:, :unit_local]) * convolved[:, unit_local:]).astype(
        jnp.bfloat16
    )
    unit_share = lax.psum_scatter(
        contract_units(hidden, collected[2]).astype(jnp.bfloat16),
        "tp",
        scatter_dimension=0,
        tiled=True,
    ).astype(jnp.float32)
    finished = (middle_rows + unit_share).astype(jnp.bfloat16)
    return lax.all_gather(finished, "tp", axis=0, tiled=True)


def solution(mesh):
    placed = (
        P("sp", None),
        P("sp", "tp"),
        P("sp", "tp"),
        P("sp", "tp"),
        P(),
        P(),
        P("tp", None),
        P(),
        P("sp", "tp"),
        P("sp", "tp"),
        P(None, "tp"),
        P(None, "tp"),
        P("sp", "tp"),
    )
    return jax.shard_map(
        shards, mesh=mesh, in_specs=placed, out_specs=P("sp", None), check_vma=False
    )
```

profile of v0, /device:TPU:0, one launch (start us, length us, event | category | flops | bytes accessed | tf_op | source)
XLA Modules:
  0.0 565.5 jit_solution(3756514513751878015)
XLA Ops:
  10.3 1.9 fusion.33
  12.2 55.7 %all-gather.6.cloned.1.call-done = bf16[2048,256]{1,0:T(8,128)(2,1)} async-done(((bf16[128,256]{1,0:T(8,128)(2,1)}), bf16[2048,256]{1,0:T(8,128)(2,1)}) %all-gather.6.cloned.1.call-update) | async-done | bytes 1048592 | tf_op jit(solution)/shard_map/all_gather | solution.py:113
  67.9 2.6 copy.18
  70.5 2.0 multiply_reduce_fusion
  73.9 7.3 %fusion.57 = (f32[4,256]{1,0:T(4,128)S(1)}, f32[4,256,2048]{2,1,0:T(8,128)S(1)}) fusion(f32[2048,4,32]{0,2,1:T(8,128)S(1)} %get-tuple-element.18, f32[2048,4,32]{0,2,1:T(8,128)S(1)} %get-tuple-element.17, f32[4,2,8,8,128]{4,3,2,1,0:T(8,128)S(1)} %bitcast.37), kind=kOutput, calls=%fused_computation.107 | convolution fusion | flops 1613233152 | bytes 10752000 | tf_op jit(solution)/shard_map/while/body/eval_jaxpr/hrd,shd->hrs/dot_general | solution.py:128
  81.3 1.3 fusion
  82.6 2.0 copy-done.2
  84.5 40.1 %all-gather.8.cloned.1.call-done = bf16[2048,256]{1,0:T(8,128)(2,1)} async-done(((bf16[128,256]{1,0:T(8,128)(2,1)}), bf16[2048,256]{1,0:T(8,128)(2,1)}) %all-gather.8.cloned.1.call-update) | async-done | bytes 1048592 | tf_op jit(solution)/shard_map/all_gather | solution.py:114
  124.6 1.7 copy.19
  126.3 4.9 fusion.21
  134.4 5.0 reduce-scatter.3.cloned.1.call-done
  141.7 2.2 all_gather.23
  143.9 130.8 %all-gather.12.cloned.1.call-done = bf16[2048,2560]{1,0:T(8,128)(2,1)} async-done(((bf16[128,2560]{1,0:T(8,128)(2,1)}), bf16[2048,2560]{1,0:T(8,128)(2,1)}) %all-gather.12.cloned.1.call-update) | async-done | bytes 10485776 | tf_op jit(solution)/shard_map/all_gather | solution.py:91
  274.6 5.5 convolution_convert_fusion
  280.2 126.7 %all-gather.10.cloned.1.call-done = bf16[2048,2560]{1,0:T(8,128)(2,1)} async-done(((bf16[128,2560]{1,0:T(8,128)(2,1)}), bf16[2048,2560]{1,0:T(8,128)(2,1)}) %all-gather.10.cloned.1.call-update) | async-done | bytes 10485776 | tf_op jit(solution)/shard_map/all_gather | solution.py:90
  406.9 5.5 convolution_convert_fusion.1
  412.4 3.4 collective-permute-start
  415.8 1.3 collective-permute-start.1
  417.4 4.6 collective-permute-done.1
  422.4 2.3 fusion.5
  424.7 114.3 %all-gather.14.cloned.1.call-done = bf16[2048,2560]{1,0:T(8,128)(2,1)} async-done(((bf16[128,2560]{1,0:T(8,128)(2,1)}), bf16[2048,2560]{1,0:T(8,128)(2,1)}) %all-gather.14.cloned.1.call-update) | async-done | bytes 10485776 | tf_op jit(solution)/shard_map/all_gather | solution.py:92
  539.1 9.2 %convolution_convert_fusion.3 = bf16[128,2048]{1,0:T(8,128)(2,1)} fusion(bf16[2048,2560]{1,0:T(8,128)(2,1)} %all-gather.14.cloned.1.call-done, f32[128,5120]{1,0:T(8,128)} %fusion.5), kind=kOutput, calls=%fused_computation.13 | convolution fusion | flops 1344405504 | bytes 13631488 | tf_op jit(solution)/shard_map/dot_general | solution.py:69
  548.3 6.3 %reduce-scatter.5.cloned.1.call-done = bf16[64,2048]{1,0:T(8,128)(2,1)} async-done(((bf16[128,2048]{1,0:T(8,128)(2,1)}), bf16[64,2048]{1,0:T(8,128)(2,1)}) %reduce-scatter.5.cloned.1.call-update) | async-done | bytes 262160 | tf_op jit(solution)/shard_map/reduce_scatter | solution.py:175
  555.6 2.2 all_gather.27
  (67 shorter events, 13.0 us)
Async XLA Ops:
  6.5 124.7 %copy-start = (bf16[512,2048]{1,0:T(8,128)(2,1)S(1)}, bf16[512,2048]{1,0:T(8,128)(2,1)}, u32[]{:S(2)}) copy-start(bf16[512,2048]{1,0:T(8,128)(2,1)} %param.19) | copy-start | bytes 6291460
  6.5 61.4 %all-gather.6.cloned.1.call-start = ((), (), s32[]{:S(2)}) async-start(), calls=%async_computation.2 | async-start | bytes 1114112 | tf_op jit(solution)/shard_map/all_gather | solution.py:113
  7.3 117.4 %all-gather.8.cloned.1.call-start = ((), (), s32[]{:S(2)}) async-start(), calls=%async_computation.3 | async-start | bytes 1114112 | tf_op jit(solution)/shard_map/all_gather | solution.py:114
  8.0 131.5 %reduce-scatter.3.cloned.1.call-start = ((), (), s32[]{:S(2)}) async-start(), calls=%async_computation.4 | async-start | bytes 786432 | tf_op jit(solution)/shard_map/reduce_scatter | solution.py:152
  12.2 60.3 %copy-start.9 = (f32[64]{0:T(128)S(1)}, f32[64]{0:T(128)}, u32[]{:S(2)}) copy-start(f32[64]{0:T(128)} %param.18) | copy-start | bytes 772
  70.5 2.2 copy-start.3
  81.3 3.3 copy-start.2
  131.2 3.1 copy-start.6
  131.2 3.2 copy-start.7
  131.2 8.2 %copy-start.5 = (bf16[128,2048]{1,0:T(8,128)(2,1)S(1)}, bf16[128,2048]{1,0:T(8,128)(2,1)}, u32[]{:S(2)}) copy-start(bf16[128,2048]{1,0:T(8,128)(2,1)} %param.13) | copy-start | bytes 1572868
  131.3 9.4 %copy-start.8 = (f32[2048]{0:T(1024)S(1)}, f32[2048]{0:T(1024)}, u32[]{:S(2)}) copy-start(f32[2048]{0:T(1024)} %param.20) | copy-start | bytes 24580
  132.6 142.1 %all-gather.12.cloned.1.call-start = ((), (), s32[]{:S(2)}) async-start(), calls=%async_computation.6 | async-start | bytes 11141120 | tf_op jit(solution)/shard_map/all_gather | solution.py:91
  133.1 273.7 %all-gather.10.cloned.1.call-start = ((), (), s32[]{:S(2)}) async-start(), calls=%async_computation.5 | async-start | bytes 11141120 | tf_op jit(solution)/shard_map/all_gather | solution.py:90
  133.7 405.4 %all-gather.14.cloned.1.call-start = ((), (), s32[]{:S(2)}) async-start(), calls=%async_computation.7 | async-start | bytes 11141120 | tf_op jit(solution)/shard_map/all_gather | solution.py:92
  134.3 420.3 %reduce-scatter.5.cloned.1.call-start = ((), (), s32[]{:S(2)}) async-start(), calls=%async_computation.8 | async-start | bytes 786432 | tf_op jit(solution)/shard_map/reduce_scatter | solution.py:175
  412.4 5.0 collective-permute-start
  415.8 6.2 %collective-permute-start.1 = (bf16[1,5120]{1,0:T(2,128)(2,1)S(1)}, bf16[1,5120]{1,0:T(2,128)(2,1)S(1)}, u32[]{:S(2)}, u32[]{:S(2)}) collective-permute-start(bf16[1,5120]{1,0:T(2,128)(2,1)S(1)} %get-tuple-element.33), channel_id=1, source_target_pairs={{2,0},{4,2},{6,4},{8,6},{10,8},{12,10},{14,12},{16,14},{18,16},{20... | collective-permute-start | bytes 30728 | tf_op jit(solution)/shard_map/ppermute | solution.py:23
  424.7 129.8 %copy-start.4 = (bf16[64,2048]{1,0:T(8,128)(2,1)S(1)}, bf16[64,2048]{1,0:T(8,128)(2,1)}, u32[]{:S(2)}) copy-start(bf16[64,2048]{1,0:T(8,128)(2,1)} %reduce-scatter.3.cloned.1.call-done) | copy-start | bytes 786436
  539.1 19.5 %copy-start.1 = (bf16[512,2048]{1,0:T(8,128)(2,1)S(1)}, bf16[512,2048]{1,0:T(8,128)(2,1)}, u32[]{:S(2)}) copy-start(bf16[512,2048]{1,0:T(8,128)(2,1)} %param.19) | copy-start | bytes 6291460
Sparse Core Ops, SparseCore 0:
  10.1 57.7 all-gather.5
  70.7 53.9 all-gather.7
  132.7 6.7 reduce-scatter.2
  142.0 132.5 all-gather.11
  277.2 129.6 all-gather.9
  409.4 129.6 all-gather.13
  548.4 6.0 reduce-scatter.4
where the time goes:
time: 566 us; the launch traced here: 565 us
  waiting for transfers between devices  487 us (86%)
  matrix products  33.7 us (6%)
  between operations  13.8 us (2%)
  other arithmetic  13.5 us (2%)
  local copies, waits for them, and re-layouts  8.35 us (1%)
    all_gather x1, waiting for transfers between devices, shards(): lax.all_gather(value_weight, 'sp', axis=0, tiled=True)  131 us
    all_gather x1, waiting for transfers between devices, shards(): lax.all_gather(gate_weight, 'sp', axis=0, tiled=True)  127 us
    all_gather x1, waiting for transfers between devices, shards(): lax.all_gather(down_weight, 'sp', axis=0, tiled=True)  114 us
    all_gather x1, waiting for transfers between devices, shards(): key_piece = lax.all_gather(keys, 'sp', axis=0, tiled=True)  55.7 us
    all_gather x1, waiting for transfers between devices, shards(): value_piece = lax.all_gather(values, 'sp', axis=0, tiled=True)  40.1 us
  transfers between devices with their start and end apart: 9, of which 9 were waited for; matrix products, arithmetic and copies ran while one was open for 6% of the time, Pallas kernels for 0%

commit v1 on v0

--- a/solution.py
+++ b/solution.py
@@ -111,7 +111,12 @@
         jnp.zeros((key_heads, lane_rows, HEAD_SIZE), jnp.float32),
     )
     key_piece = lax.all_gather(keys, "sp", axis=0, tiled=True)
-    value_piece = lax.all_gather(values, "sp", axis=0, tiled=True)
+    ring = [values]
+    for hop in range(15):
+        ring.append(lax.ppermute(ring[-1], "sp", [(dev, (dev + 1) % 16) for dev in range(16)]))
+    value_piece = jnp.roll(
+        jnp.concatenate(ring[::-1], axis=0), (lax.axis_index("sp") + 1) * ring[0].shape[0], axis=0
+    )
     row_count = key_piece.shape[0]
     key_places = jnp.arange(row_count, dtype=jnp.int32)
     turned = apply_rotary(

time: 566 us -> 589 us (1.041)
  waiting for transfers between devices: 487 us -> 500 us
  local copies, waits for them, and re-layouts: 8.35 us -> 14.6 us
    ppermute x0 -> x15, waiting for transfers between devices: none -> 113 us  [shards(): lax.ppermute(ring[-1], 'sp', [(dev, (dev + 1) % 16) for dev in range(16)])]
    all_gather x1, waiting for transfers between devices: 55.7 us -> 0.02 us  [shards(): key_piece = lax.all_gather(keys, 'sp', axis=0, tiled=True)]
    all_gather x1 -> x0, waiting for transfers between devices: 40.1 us -> none  [shards(): value_piece = lax.all_gather(values, 'sp', axis=0, tiled=True)]
  transfers between devices with their start and end apart: 9 -> 23, of which waited for: 9 -> 22; matrix products, arithmetic and copies ran while one was open for 6% -> 5% of each run, Pallas kernels for 0% -> 0%
where the time goes in v1:
time: 589 us; the launch traced here: 588 us
  waiting for transfers between devices  500 us (85%)
  matrix products  30.4 us (5%)
  other arithmetic  16.6 us (3%)
  local copies, waits for them, and re-layouts  14.6 us (2%)
  between operations  14 us (2%)
  starting transfers between devices  8.11 us (1%)
    all_gather x1, waiting for transfers between devices, shards(): lax.all_gather(value_weight, 'sp', axis=0, tiled=True)  131 us
    all_gather x1, waiting for transfers between devices, shards(): lax.all_gather(gate_weight, 'sp', axis=0, tiled=True)  127 us
    all_gather x1, waiting for transfers between devices, shards(): lax.all_gather(down_weight, 'sp', axis=0, tiled=True)  114 us
    ppermute x15, waiting for transfers between devices, shards(): lax.ppermute(ring[-1], 'sp', [(dev, (dev + 1) % 16) for dev in range(16)])  113 us
  transfers between devices with their start and end apart: 23, of which 22 were waited for; matrix products, arithmetic and copies ran while one was open for 5% of the time, Pallas kernels for 0%

profile of v1, /device:TPU:0, one launch (start us, length us, event | category | flops | bytes accessed | tf_op | source)
XLA Modules:
  0.0 588.5 jit_solution(12251099008002264862)
XLA Ops:
  10.3 6.4 %collective-permute-done = bf16[128,256]{1,0:T(8,128)(2,1)S(1)} collective-permute-done((bf16[128,256]{1,0:T(8,128)(2,1)}, bf16[128,256]{1,0:T(8,128)(2,1)S(1)}, u32[]{:S(2)}, u32[]{:S(2)}) %collective-permute-start) | collective-permute-done | bytes 65568 | tf_op jit(solution)/shard_map/ppermute | solution.py:116
  16.8 7.9 %collective-permute-done.1 = bf16[128,256]{1,0:T(8,128)(2,1)S(1)} collective-permute-done((bf16[128,256]{1,0:T(8,128)(2,1)S(1)}, bf16[128,256]{1,0:T(8,128)(2,1)S(1)}, u32[]{:S(2)}, u32[]{:S(2)}) %collective-permute-start.1) | collective-permute-done | bytes 65568 | tf_op jit(solution)/shard_map/ppermute | solution.py:116
  24.7 7.9 %collective-permute-done.2 = bf16[128,256]{1,0:T(8,128)(2,1)S(1)} collective-permute-done((bf16[128,256]{1,0:T(8,128)(2,1)S(1)}, bf16[128,256]{1,0:T(8,128)(2,1)S(1)}, u32[]{:S(2)}, u32[]{:S(2)}) %collective-permute-start.2) | collective-permute-done | bytes 65568 | tf_op jit(solution)/shard_map/ppermute | solution.py:116
  32.7 7.9 %collective-permute-done.3 = bf16[128,256]{1,0:T(8,128)(2,1)S(1)} collective-permute-done((bf16[128,256]{1,0:T(8,128)(2,1)S(1)}, bf16[128,256]{1,0:T(8,128)(2,1)S(1)}, u32[]{:S(2)}, u32[]{:S(2)}) %collective-permute-start.3) | collective-permute-done | bytes 65568 | tf_op jit(solution)/shard_map/ppermute | solution.py:116
  44.2 4.5 collective-permute-done.4
  48.7 8.6 %collective-permute-done.5 = bf16[128,256]{1,0:T(8,128)(2,1)S(1)} collective-permute-done((bf16[128,256]{1,0:T(8,128)(2,1)S(1)}, bf16[128,256]{1,0:T(8,128)(2,1)S(1)}, u32[]{:S(2)}, u32[]{:S(2)}) %collective-permute-start.5) | collective-permute-done | bytes 65568 | tf_op jit(solution)/shard_map/ppermute | solution.py:116
  57.2 9.3 %collective-permute-done.6 = bf16[128,256]{1,0:T(8,128)(2,1)S(1)} collective-permute-done((bf16[128,256]{1,0:T(8,128)(2,1)S(1)}, bf16[128,256]{1,0:T(8,128)(2,1)S(1)}, u32[]{:S(2)}, u32[]{:S(2)}) %collective-permute-start.6) | collective-permute-done | bytes 65568 | tf_op jit(solution)/shard_map/ppermute | solution.py:116
  67.3 7.1 %collective-permute-done.7 = bf16[128,256]{1,0:T(8,128)(2,1)S(1)} collective-permute-done((bf16[128,256]{1,0:T(8,128)(2,1)S(1)}, bf16[128,256]{1,0:T(8,128)(2,1)S(1)}, u32[]{:S(2)}, u32[]{:S(2)}) %collective-permute-start.7) | collective-permute-done | bytes 65568 | tf_op jit(solution)/shard_map/ppermute | solution.py:116
  75.1 7.1 %collective-permute-done.8 = bf16[128,256]{1,0:T(8,128)(2,1)S(1)} collective-permute-done((bf16[128,256]{1,0:T(8,128)(2,1)S(1)}, bf16[128,256]{1,0:T(8,128)(2,1)S(1)}, u32[]{:S(2)}, u32[]{:S(2)}) %collective-permute-start.8) | collective-permute-done | bytes 65568 | tf_op jit(solution)/shard_map/ppermute | solution.py:116
  82.2 7.8 %collective-permute-done.9 = bf16[128,256]{1,0:T(8,128)(2,1)S(1)} collective-permute-done((bf16[128,256]{1,0:T(8,128)(2,1)S(1)}, bf16[128,256]{1,0:T(8,128)(2,1)S(1)}, u32[]{:S(2)}, u32[]{:S(2)}) %collective-permute-start.9) | collective-permute-done | bytes 65568 | tf_op jit(solution)/shard_map/ppermute | solution.py:116
  90.2 7.8 %collective-permute-done.10 = bf16[128,256]{1,0:T(8,128)(2,1)S(1)} collective-permute-done((bf16[128,256]{1,0:T(8,128)(2,1)S(1)}, bf16[128,256]{1,0:T(8,128)(2,1)S(1)}, u32[]{:S(2)}, u32[]{:S(2)}) %collective-permute-start.10) | collective-permute-done | bytes 65568 | tf_op jit(solution)/shard_map/ppermute | solution.py:116
  98.0 7.8 %collective-permute-done.11 = bf16[128,256]{1,0:T(8,128)(2,1)S(1)} collective-permute-done((bf16[128,256]{1,0:T(8,128)(2,1)S(1)}, bf16[128,256]{1,0:T(8,128)(2,1)S(1)}, u32[]{:S(2)}, u32[]{:S(2)}) %collective-permute-start.11) | collective-permute-done | bytes 65568 | tf_op jit(solution)/shard_map/ppermute | solution.py:116
  105.9 8.4 %collective-permute-done.12 = bf16[128,256]{1,0:T(8,128)(2,1)} collective-permute-done((bf16[128,256]{1,0:T(8,128)(2,1)S(1)}, bf16[128,256]{1,0:T(8,128)(2,1)}, u32[]{:S(2)}, u32[]{:S(2)}) %collective-permute-start.12) | collective-permute-done | bytes 65568 | tf_op jit(solution)/shard_map/ppermute | solution.py:116
  115.4 7.1 %collective-permute-done.13 = bf16[128,256]{1,0:T(8,128)(2,1)} collective-permute-done((bf16[128,256]{1,0:T(8,128)(2,1)}, bf16[128,256]{1,0:T(8,128)(2,1)}, u32[]{:S(2)}, u32[]{:S(2)}) %collective-permute-start.13) | collective-permute-done | bytes 65568 | tf_op jit(solution)/shard_map/ppermute | solution.py:116
  123.3 7.3 %collective-permute-done.14 = bf16[128,256]{1,0:T(8,128)(2,1)S(1)} collective-permute-done((bf16[128,256]{1,0:T(8,128)(2,1)}, bf16[128,256]{1,0:T(8,128)(2,1)S(1)}, u32[]{:S(2)}, u32[]{:S(2)}) %collective-permute-start.14) | collective-permute-done | bytes 65568 | tf_op jit(solution)/shard_map/ppermute | solution.py:116
  146.8 7.3 %fusion.57 = (f32[4,256]{1,0:T(4,128)S(1)}, f32[4,256,2048]{2,1,0:T(8,128)S(1)}) fusion(f32[2048,4,32]{0,2,1:T(8,128)S(1)} %get-tuple-element.18, f32[2048,4,32]{0,2,1:T(8,128)S(1)} %get-tuple-element.17, f32[4,2,8,8,128]{4,3,2,1,0:T(8,128)S(1)} %bitcast.37), kind=kOutput, calls=%fused_computation.140 | convolution fusion | flops 1613233152 | bytes 10752000 | tf_op jit(solution)/shard_map/while/body/eval_jaxpr/hrd,shd->hrs/dot_general | solution.py:133
  166.8 130.9 %all-gather.9.cloned.1.call-done = bf16[2048,2560]{1,0:T(8,128)(2,1)} async-done(((bf16[128,2560]{1,0:T(8,128)(2,1)}), bf16[2048,2560]{1,0:T(8,128)(2,1)}) %all-gather.9.cloned.1.call-update) | async-done | bytes 10485776 | tf_op jit(solution)/shard_map/all_gather | solution.py:91
  297.7 5.5 convolution_convert_fusion
  303.2 126.7 %all-gather.7.cloned.1.call-done = bf16[2048,2560]{1,0:T(8,128)(2,1)} async-done(((bf16[128,2560]{1,0:T(8,128)(2,1)}), bf16[2048,2560]{1,0:T(8,128)(2,1)}) %all-gather.7.cloned.1.call-update) | async-done | bytes 10485776 | tf_op jit(solution)/shard_map/all_gather | solution.py:90
  429.9 5.5 convolution_convert_fusion.1
  440.5 4.6 collective-permute-done.16
  447.8 114.3 %all-gather.11.cloned.1.call-done = bf16[2048,2560]{1,0:T(8,128)(2,1)} async-done(((bf16[128,2560]{1,0:T(8,128)(2,1)}), bf16[2048,2560]{1,0:T(8,128)(2,1)}) %all-gather.11.cloned.1.call-update) | async-done | bytes 10485776 | tf_op jit(solution)/shard_map/all_gather | solution.py:92
  562.1 9.2 %convolution_convert_fusion.3 = bf16[128,2048]{1,0:T(8,128)(2,1)} fusion(bf16[2048,2560]{1,0:T(8,128)(2,1)} %all-gather.11.cloned.1.call-done, f32[128,5120]{1,0:T(8,128)} %fusion.5), kind=kOutput, calls=%fused_computation.13 | convolution fusion | flops 1344405504 | bytes 13631488 | tf_op jit(solution)/shard_map/dot_general | solution.py:69
  571.3 6.3 %reduce-scatter.5.cloned.1.call-done = bf16[64,2048]{1,0:T(8,128)(2,1)} async-done(((bf16[128,2048]{1,0:T(8,128)(2,1)}), bf16[64,2048]{1,0:T(8,128)(2,1)}) %reduce-scatter.5.cloned.1.call-update) | async-done | bytes 262160 | tf_op jit(solution)/shard_map/reduce_scatter | solution.py:180
  (147 shorter events, 51.1 us)
Async XLA Ops:
  6.5 150.5 %copy-start = (bf16[512,2048]{1,0:T(8,128)(2,1)S(1)}, bf16[512,2048]{1,0:T(8,128)(2,1)}, u32[]{:S(2)}) copy-start(bf16[512,2048]{1,0:T(8,128)(2,1)} %param.19) | copy-start | bytes 6291460
  6.5 133.0 %all-gather.5.cloned.1.call-start = ((), (), s32[]{:S(2)}) async-start(), calls=%async_computation.2 | async-start | bytes 1114112 | tf_op jit(solution)/shard_map/all_gather | solution.py:113
  7.3 155.1 %reduce-scatter.3.cloned.1.call-start = ((), (), s32[]{:S(2)}) async-start(), calls=%async_computation.3 | async-start | bytes 786432 | tf_op jit(solution)/shard_map/reduce_scatter | solution.py:157
  7.3 9.5 %collective-permute-start = (bf16[128,256]{1,0:T(8,128)(2,1)}, bf16[128,256]{1,0:T(8,128)(2,1)S(1)}, u32[]{:S(2)}, u32[]{:S(2)}) collective-permute-start(bf16[128,256]{1,0:T(8,128)(2,1)} %param.16), channel_id=1, source_target_pairs={{0,2},{2,4},{4,6},{6,8},{8,10},{10,12},{12,14},{14,16},{16,18},{18... | collective-permute-start | bytes 196616 | tf_op jit(solution)/shard_map/ppermute | solution.py:116
  16.8 7.9 %collective-permute-start.1 = (bf16[128,256]{1,0:T(8,128)(2,1)S(1)}, bf16[128,256]{1,0:T(8,128)(2,1)S(1)}, u32[]{:S(2)}, u32[]{:S(2)}) collective-permute-start(bf16[128,256]{1,0:T(8,128)(2,1)S(1)} %collective-permute-done), channel_id=1, source_target_pairs={{0,2},{2,4},{4,6},{6,8},{8,10},{10,12},{12,14},{14,16},{16,18},{18... | collective-permute-start | bytes 196616 | tf_op jit(solution)/shard_map/ppermute | solution.py:116
  24.7 7.9 %collective-permute-start.2 = (bf16[128,256]{1,0:T(8,128)(2,1)S(1)}, bf16[128,256]{1,0:T(8,128)(2,1)S(1)}, u32[]{:S(2)}, u32[]{:S(2)}) collective-permute-start(bf16[128,256]{1,0:T(8,128)(2,1)S(1)} %collective-permute-done.1), channel_id=1, source_target_pairs={{0,2},{2,4},{4,6},{6,8},{8,10},{10,12},{12,14},{14,16},{16,18},{18... | collective-permute-start | bytes 196616 | tf_op jit(solution)/shard_map/ppermute | solution.py:116
  32.6 8.0 %collective-permute-start.3 = (bf16[128,256]{1,0:T(8,128)(2,1)S(1)}, bf16[128,256]{1,0:T(8,128)(2,1)S(1)}, u32[]{:S(2)}, u32[]{:S(2)}) collective-permute-start(bf16[128,256]{1,0:T(8,128)(2,1)S(1)} %collective-permute-done.2), channel_id=1, source_target_pairs={{0,2},{2,4},{4,6},{6,8},{8,10},{10,12},{12,14},{14,16},{16,18},{18... | collective-permute-start | bytes 196616 | tf_op jit(solution)/shard_map/ppermute | solution.py:116
  40.6 8.0 %collective-permute-start.4 = (bf16[128,256]{1,0:T(8,128)(2,1)S(1)}, bf16[128,256]{1,0:T(8,128)(2,1)S(1)}, u32[]{:S(2)}, u32[]{:S(2)}) collective-permute-start(bf16[128,256]{1,0:T(8,128)(2,1)S(1)} %collective-permute-done.3), channel_id=1, source_target_pairs={{0,2},{2,4},{4,6},{6,8},{8,10},{10,12},{12,14},{14,16},{16,18},{18... | collective-permute-start | bytes 196616 | tf_op jit(solution)/shard_map/ppermute | solution.py:116
  48.6 8.6 %collective-permute-start.5 = (bf16[128,256]{1,0:T(8,128)(2,1)S(1)}, bf16[128,256]{1,0:T(8,128)(2,1)S(1)}, u32[]{:S(2)}, u32[]{:S(2)}) collective-permute-start(bf16[128,256]{1,0:T(8,128)(2,1)S(1)} %collective-permute-done.4), channel_id=1, source_target_pairs={{0,2},{2,4},{4,6},{6,8},{8,10},{10,12},{12,14},{14,16},{16,18},{18... | collective-permute-start | bytes 196616 | tf_op jit(solution)/shard_map/ppermute | solution.py:116
  57.2 9.3 %collective-permute-start.6 = (bf16[128,256]{1,0:T(8,128)(2,1)S(1)}, bf16[128,256]{1,0:T(8,128)(2,1)S(1)}, u32[]{:S(2)}, u32[]{:S(2)}) collective-permute-start(bf16[128,256]{1,0:T(8,128)(2,1)S(1)} %collective-permute-done.5), channel_id=1, source_target_pairs={{0,2},{2,4},{4,6},{6,8},{8,10},{10,12},{12,14},{14,16},{16,18},{18... | collective-permute-start | bytes 196616 | tf_op jit(solution)/shard_map/ppermute | solution.py:116
  66.5 7.9 %collective-permute-start.7 = (bf16[128,256]{1,0:T(8,128)(2,1)S(1)}, bf16[128,256]{1,0:T(8,128)(2,1)S(1)}, u32[]{:S(2)}, u32[]{:S(2)}) collective-permute-start(bf16[128,256]{1,0:T(8,128)(2,1)S(1)} %collective-permute-done.6), channel_id=1, source_target_pairs={{0,2},{2,4},{4,6},{6,8},{8,10},{10,12},{12,14},{14,16},{16,18},{18... | collective-permute-start | bytes 196616 | tf_op jit(solution)/shard_map/ppermute | solution.py:116
  74.4 7.9 %collective-permute-start.8 = (bf16[128,256]{1,0:T(8,128)(2,1)S(1)}, bf16[128,256]{1,0:T(8,128)(2,1)S(1)}, u32[]{:S(2)}, u32[]{:S(2)}) collective-permute-start(bf16[128,256]{1,0:T(8,128)(2,1)S(1)} %collective-permute-done.7), channel_id=1, source_target_pairs={{0,2},{2,4},{4,6},{6,8},{8,10},{10,12},{12,14},{14,16},{16,18},{18... | collective-permute-start | bytes 196616 | tf_op jit(solution)/shard_map/ppermute | solution.py:116
  82.2 7.9 %collective-permute-start.9 = (bf16[128,256]{1,0:T(8,128)(2,1)S(1)}, bf16[128,256]{1,0:T(8,128)(2,1)S(1)}, u32[]{:S(2)}, u32[]{:S(2)}) collective-permute-start(bf16[128,256]{1,0:T(8,128)(2,1)S(1)} %collective-permute-done.8), channel_id=1, source_target_pairs={{0,2},{2,4},{4,6},{6,8},{8,10},{10,12},{12,14},{14,16},{16,18},{18... | collective-permute-start | bytes 196616 | tf_op jit(solution)/shard_map/ppermute | solution.py:116
  90.1 7.9 %collective-permute-start.10 = (bf16[128,256]{1,0:T(8,128)(2,1)S(1)}, bf16[128,256]{1,0:T(8,128)(2,1)S(1)}, u32[]{:S(2)}, u32[]{:S(2)}) collective-permute-start(bf16[128,256]{1,0:T(8,128)(2,1)S(1)} %collective-permute-done.9), channel_id=1, source_target_pairs={{0,2},{2,4},{4,6},{6,8},{8,10},{10,12},{12,14},{14,16},{16,18},{18... | collective-permute-start | bytes 196616 | tf_op jit(solution)/shard_map/ppermute | solution.py:116
  98.0 7.9 %collective-permute-start.11 = (bf16[128,256]{1,0:T(8,128)(2,1)S(1)}, bf16[128,256]{1,0:T(8,128)(2,1)S(1)}, u32[]{:S(2)}, u32[]{:S(2)}) collective-permute-start(bf16[128,256]{1,0:T(8,128)(2,1)S(1)} %collective-permute-done.10), channel_id=1, source_target_pairs={{0,2},{2,4},{4,6},{6,8},{8,10},{10,12},{12,14},{14,16},{16,18},{18... | collective-permute-start | bytes 196616 | tf_op jit(solution)/shard_map/ppermute | solution.py:116
  105.9 8.5 %collective-permute-start.12 = (bf16[128,256]{1,0:T(8,128)(2,1)S(1)}, bf16[128,256]{1,0:T(8,128)(2,1)}, u32[]{:S(2)}, u32[]{:S(2)}) collective-permute-start(bf16[128,256]{1,0:T(8,128)(2,1)S(1)} %collective-permute-done.11), channel_id=1, source_target_pairs={{0,2},{2,4},{4,6},{6,8},{8,10},{10,12},{12,14},{14,16},{16,18},{18... | collective-permute-start | bytes 196616 | tf_op jit(solution)/shard_map/ppermute | solution.py:116
  114.4 8.2 %collective-permute-start.13 = (bf16[128,256]{1,0:T(8,128)(2,1)}, bf16[128,256]{1,0:T(8,128)(2,1)}, u32[]{:S(2)}, u32[]{:S(2)}) collective-permute-start(bf16[128,256]{1,0:T(8,128)(2,1)} %collective-permute-done.12), channel_id=1, source_target_pairs={{0,2},{2,4},{4,6},{6,8},{8,10},{10,12},{12,14},{14,16},{16,18},{18... | collective-permute-start | bytes 196616 | tf_op jit(solution)/shard_map/ppermute | solution.py:116
  122.5 8.1 %collective-permute-start.14 = (bf16[128,256]{1,0:T(8,128)(2,1)}, bf16[128,256]{1,0:T(8,128)(2,1)S(1)}, u32[]{:S(2)}, u32[]{:S(2)}) collective-permute-start(bf16[128,256]{1,0:T(8,128)(2,1)} %collective-permute-done.13), channel_id=1, source_target_pairs={{0,2},{2,4},{4,6},{6,8},{8,10},{10,12},{12,14},{14,16},{16,18},{18... | collective-permute-start | bytes 196616 | tf_op jit(solution)/shard_map/ppermute | solution.py:116
  158.4 139.3 %all-gather.9.cloned.1.call-start = ((), (), s32[]{:S(2)}) async-start(), calls=%async_computation.5 | async-start | bytes 11141120 | tf_op jit(solution)/shard_map/all_gather | solution.py:91
  159.1 270.8 %all-gather.7.cloned.1.call-start = ((), (), s32[]{:S(2)}) async-start(), calls=%async_computation.4 | async-start | bytes 11141120 | tf_op jit(solution)/shard_map/all_gather | solution.py:90
  159.7 402.4 %all-gather.11.cloned.1.call-start = ((), (), s32[]{:S(2)}) async-start(), calls=%async_computation.6 | async-start | bytes 11141120 | tf_op jit(solution)/shard_map/all_gather | solution.py:92
  160.3 417.3 %reduce-scatter.5.cloned.1.call-start = ((), (), s32[]{:S(2)}) async-start(), calls=%async_computation.7 | async-start | bytes 786432 | tf_op jit(solution)/shard_map/reduce_scatter | solution.py:180
  435.5 5.0 collective-permute-start.15
  438.8 6.2 %collective-permute-start.16 = (bf16[1,5120]{1,0:T(2,128)(2,1)S(1)}, bf16[1,5120]{1,0:T(2,128)(2,1)S(1)}, u32[]{:S(2)}, u32[]{:S(2)}) collective-permute-start(bf16[1,5120]{1,0:T(2,128)(2,1)S(1)} %get-tuple-element.33), channel_id=1, source_target_pairs={{2,0},{4,2},{6,4},{8,6},{10,8},{12,10},{14,12},{16,14},{18,16},{20... | collective-permute-start | bytes 30728 | tf_op jit(solution)/shard_map/ppermute | solution.py:23
  (19 other events, 358.5 us)
Sparse Core Ops, SparseCore 0:
  10.1 59.4 all-gather.4
  158.5 3.7 reduce-scatter.2
  165.1 132.5 all-gather.8
  300.2 129.6 all-gather.6
  432.4 129.6 all-gather.10
  571.5 6.0 reduce-scatter.4
